TPU v7x, 32 devices: a whole 2x2x4 slice. The times are simulated.
32 devices in a mesh: grp: 2 (over y), kv: 4 (over z), tp: 4 (over x, core).
Axes of the slice: x: 2, y: 2, z: 4, core: 2. Of those that a mesh axis runs over, the one named last changes fastest.
Arguments:
- stream: bfloat16 [16, 4096], P('grp', 'kv'), parts along dimension 0, may hold values from -6 to 6
- attn_gain: bfloat16 [4096], P('kv'), may hold values from 0.099609375 to 1.8984375
- query_weight: bfloat16 [4096, 4096], P('kv', 'tp'), may hold values from -0.09375 to 0.09375
- query_gain: float32 [64], replicated, may hold values from 0.1 to 1.9
- key_cache: bfloat16 [16, 2048, 1024], P('grp', 'kv', 'tp'), parts along dimension 0, may hold values from -200 to 200
- value_cache: bfloat16 [16, 2048, 1024], P('grp', 'kv', 'tp'), parts along dimension 0, may hold values from -6 to 6
- gate_cache: float32 [16, 16, 2048], P('grp', 'tp', 'kv'), parts along dimension 0, may hold values from -2048 to 0, as said below
- output_weight: bfloat16 [4096, 4096], P('tp', 'kv'), may hold values from -0.75 to 0.75
- mixer_gain: bfloat16 [4096], replicated, may hold values from 0.099609375 to 1.8984375
- up_weight: bfloat16 [16384, 4096], P(('kv', 'tp')), may hold values from -0.09375 to 0.09375
- down_weight: bfloat16 [16384, 4096], P(('kv', 'tp')), may hold values from -0.0625 to 0.0625
Outputs:
- result: bfloat16 [16, 4096], P('grp', ('kv', 'tp')), parts along dimension 0
There are 2 independent parts, one for each index of `grp`. A program takes and returns all parts, laid end to end along the dimension named above; an argument that names none is the same for every part. Nothing has to cross between parts.
Inputs may be any that keep to these rules, and one draw needn't show every extreme that they name: `gate_cache`: cumulative log forget gates: along positions each row never rises.
All inputs are finite; a program needn't handle non-finite values.
Results may differ from a plain program's by a relative error of at most 0.007.
The roundings to bfloat16 on the way count: a program that leaves them out, or rounds other values in their place, can miss the bound.
Values may be sent and summed in bfloat16 or wider, within the bound.
No kernel may reach another device: no remote copies, remote signals or barrier semaphores. Data moves between devices by JAX's collectives and lax.ppermute only.
A program may use at most 64 MiB of HBM per device.

v0:
```python
import jax
import jax.numpy as jnp
from jax import lax
from jax.sharding import PartitionSpec as P

HEAD_DIM = 64
EPS = 1e-06


def rms_scale(values):
    return lax.rsqrt(jnp.mean(values * values, axis=-1, keepdims=True) + EPS)


def block_attention(queries, key_block, value_block, gate_block):
    batch_rows, position_index = (key_block.shape[0], key_block.shape[1])
    kv_local = queries.shape[1]
    key_heads = key_block.reshape(batch_rows, position_index, kv_local, HEAD_DIM)
    value_heads = value_block.reshape(batch_rows, position_index, kv_local, HEAD_DIM)
    scores = jnp.einsum("skgd,spkd->skgp", queries, key_heads, preferred_element_type=jnp.float32)
    scores = scores * HEAD_DIM ** (-0.5) - gate_block[:, :, None, :]
    score_top = jnp.max(scores, axis=-1)
    weights_exp = jnp.exp(scores - score_top[..., None])
    totals = jnp.sum(weights_exp, axis=-1)
    weighted = jnp.einsum(
        "skgp,spkd->skgd",
        weights_exp.astype(jnp.bfloat16),
        value_heads,
        preferred_element_type=jnp.float32,
    )
    return (score_top, totals, weighted)


def per_device(
    stream,
    attn_gain,
    query_weight,
    query_gain,
    key_cache,
    value_cache,
    gate_cache,
    output_weight,
    mixer_gain,
    up_weight,
    down_weight,
):
    batch_rows = stream.shape[0]
    scaled = (stream.astype(jnp.float32) * attn_gain.astype(jnp.float32)).astype(jnp.bfloat16)
    partial_value = jnp.dot(scaled, query_weight, preferred_element_type=jnp.float32)
    query_raw = lax.psum(partial_value, "kv")
    kv_local = key_cache.shape[2] // HEAD_DIM
    heads_local = query_raw.shape[1] // HEAD_DIM
    query_heads = query_raw.reshape(batch_rows, heads_local, HEAD_DIM)
    queries = (query_heads * rms_scale(query_heads) * query_gain).astype(jnp.bfloat16)
    queries = queries.reshape(batch_rows, kv_local, heads_local // kv_local, HEAD_DIM)
    score_top, totals, weighted = block_attention(queries, key_cache, value_cache, gate_cache)
    best = lax.pmax(score_top, "kv")
    factor = jnp.exp(score_top - best)
    totals, weighted = lax.psum((factor * totals, factor[..., None] * weighted), "kv")
    attended = (weighted / totals[..., None]).reshape(batch_rows, heads_local * HEAD_DIM)
    attended = attended.astype(jnp.bfloat16)
    projected = jnp.dot(attended, output_weight, preferred_element_type=jnp.float32)
    projected = lax.psum_scatter(projected, "tp", scatter_dimension=1, tiled=True)
    slice_width = projected.shape[1]
    own_slice = lax.dynamic_slice_in_dim(stream, lax.axis_index("tp") * slice_width, slice_width, 1)
    residual = (own_slice.astype(jnp.float32) + projected).astype(jnp.bfloat16)
    full_rows = lax.all_gather(residual, ("kv", "tp"), axis=1, tiled=True).astype(jnp.float32)
    normed = (full_rows * rms_scale(full_rows) * mixer_gain.astype(jnp.float32)).astype(
        jnp.bfloat16
    )
    up_proj = lax.dot_general(
        normed, up_weight, (((1,), (1,)), ((), ())), preferred_element_type=jnp.float32
    )
    squared = jnp.square(jax.nn.relu(up_proj)).astype(jnp.bfloat16)
    partials = jnp.dot(squared, down_weight, preferred_element_type=jnp.float32)
    summed = lax.psum_scatter(partials, ("kv", "tp"), scatter_dimension=1, tiled=True)
    return (residual.astype(jnp.float32) + summed).astype(jnp.bfloat16)


def solution(mesh):
    in_specs = (
        P("grp", "kv"),
        P("kv"),
        P("kv", "tp"),
        P(),
        P("grp", "kv", "tp"),
        P("grp", "kv", "tp"),
        P("grp", "tp", "kv"),
        P("tp", "kv"),
        P(),
        P(("kv", "tp"), None),
        P(("kv", "tp"), None),
    )
    out_specs = P("grp", ("kv", "tp"))
    return jax.shard_map(
        per_device, mesh=mesh, in_specs=in_specs, out_specs=out_specs, check_vma=False
    )
```

profile of v0, /device:TPU:0, one launch (start us, length us, event | category | flops | bytes accessed | tf_op | source)
XLA Modules:
  0.0 189.7 jit_solution(11805961911175229180)
XLA Ops:
  6.5 0.0 copy-start
  6.5 0.0 reduce-scatter.3.cloned.1.call-start
  6.5 0.8 convert_element_type.48
  7.4 0.8 copy-done
  8.1 1.1 fusion.19
  9.2 20.8 %psum.21 = f32[8,1024]{1,0:T(8,128)S(1)} all-reduce(f32[8,1024]{1,0:T(8,128)S(1)} %fusion.19), channel_id=1, replica_groups=mesh['grp'=2,'kv'=4,'tp'=4] {'kv'}, use_global_device_ids=true, to_apply=%region_0.0 | all-reduce | flops 8192 | bytes 65536 | tf_op jit(solution)/shard_map/psum | solution.py:49
  30.1 0.1 reshape.45
  30.2 0.1 mul.75
  30.2 0.1 reduce_sum.27
  30.4 0.1 copy.18
  30.4 0.1 copy.19
  30.5 4.0 %copy.20 = bf16[8,512,256]{1,2,0:T(8,128)(2,1)} copy(bf16[8,512,256]{2,1,0:T(8,128)(2,1)} %param.15) | data formatting | bytes 4194304 | tf_op args[4]
  34.5 2.1 %fusion.24 = (f32[8,4,4]{2,1,0:T(4,128)S(1)}, f32[8,4,4,512]{3,2,1,0:T(4,128)S(1)}) fusion(f32[8,4,512]{2,1,0:T(4,128)S(1)} %copy-done.1, bf16[8,512,4,64]{1,3,2,0:T(8,128)(2,1)} %bitcast.15, f32[8,4,4,64]{3,2,1,0:T(4,128)S(1)} %reshape.45, f32[64]{0:T(128)S(1)} %copy-done.3, f32[8,4,4]{2,1,0:T(4,128)S(1)} %copy.19), kind=kOutput, calls=%fused_computation.33 | convolution fusion | flops 8609664 | bytes 2458880 | tf_op jit(solution)/shard_map/skgd,spkd->skgp/dot_general | solution.py:19
  36.6 15.5 %pmax.7 = f32[8,4,4]{2,1,0:T(4,128)S(1)} all-reduce(f32[8,4,4]{2,1,0:T(4,128)S(1)} %get-tuple-element.9), channel_id=1, replica_groups=mesh['grp'=2,'kv'=4,'tp'=4] {'kv'}, use_global_device_ids=true, to_apply=%region_3.0 | all-reduce | flops 128 | bytes 1024 | tf_op jit(solution)/shard_map/pmax | solution.py:56
  52.2 0.2 fusion.4
  52.4 3.9 %copy.21 = bf16[8,512,256]{1,2,0:T(8,128)(2,1)} copy(bf16[8,512,256]{2,1,0:T(8,128)(2,1)} %param.16) | data formatting | bytes 4194304 | tf_op args[5]
  56.4 0.0 copy-start.2
  56.4 2.3 %convolution_multiply_fusion.1 = f32[8,4,4,64]{3,2,1,0:T(4,128)S(1)} fusion(bf16[8,512,4,64]{1,3,2,0:T(8,128)(2,1)} %bitcast.16, f32[8,4,4,512]{3,2,1,0:T(4,128)S(1)} %get-tuple-element.10, f32[8,4,4]{2,1,0:T(4,128)S(1)} %get-tuple-element.9, f32[8,4,4]{2,1,0:T(4,128)S(1)} %bitcast.22), kind=kOutput, calls=%fused_computation.2 | convolution fusion | flops 8527872 | bytes 2393088 | tf_op jit(solution)/shard_map/skgp,spkd->skgd/dot_general | solution.py:24
  58.7 17.6 %all-reduce = (f32[8,4,4,64]{3,2,1,0:T(4,128)S(1)}, f32[8,4,4]{2,1,0:T(4,128)S(1)}) all-reduce(f32[8,4,4,64]{3,2,1,0:T(4,128)S(1)} %convolution_multiply_fusion.1, f32[8,4,4]{2,1,0:T(4,128)S(1)} %bitcast.18), channel_id=1, replica_groups=mesh['grp'=2,'kv'=4,'tp'=4] {'kv'}, use_global_device_ids=true, to_apply=%region_4.0 | all-reduce | flops 8320 | bytes 66560 | tf_op jit(solution)/shard_map/psum | solution.py:58
  76.3 0.1 divide_convert_fusion
  76.4 0.1 convert_element_type.53
  76.5 2.6 %fusion.25 = f32[8,1024]{1,0:T(8,128)} fusion(bf16[8,1024]{1,0:T(8,128)(2,1)S(1)} %convert_element_type.53, bf16[1024,1024]{1,0:T(8,128)(2,1)} %param.18), kind=kOutput, calls=%fused_computation.34 | convolution fusion | flops 16777216 | bytes 2146304 | tf_op jit(solution)/shard_map/dot_general | solution.py:61
  79.1 0.0 reduce-scatter.3.cloned.1.call-update
  79.1 0.0 reduce-scatter.5.cloned.1.call-start
  79.2 18.2 %reduce-scatter.3.cloned.1.call-done = f32[8,256]{1,0:T(8,128)} async-done(((f32[8,1024]{1,0:T(8,128)}), f32[8,256]{1,0:T(8,128)}) %reduce-scatter.3.cloned.1.call-update) | async-done | bytes 8208 | tf_op jit(solution)/shard_map/reduce_scatter | solution.py:62
  97.4 0.7 add_convert_fusion.1
  98.1 20.6 %all_gather.3 = bf16[8,4096]{1,0:T(8,128)(2,1)S(1)} all-gather(bf16[8,256]{1,0:T(8,128)(2,1)S(1)} %add_convert_fusion.1), channel_id=1, replica_groups=mesh['grp'=2,'kv'=4,'tp'=4] {'kv','tp'}, dimensions={1}, use_global_device_ids=true | all-gather | bytes 69632 | tf_op jit(solution)/shard_map/all_gather | solution.py:66
  118.7 0.1 fusion.6
  118.8 9.8 %fusion.3 = f32[8,4096]{1,0:T(8,128)} fusion(bf16[1024,4096]{1,0:T(8,128)(2,1)} %param.21, bf16[1024,4096]{1,0:T(8,128)(2,1)} %param.20, bf16[8,4096]{1,0:T(8,128)(2,1)S(1)} %all_gather.3, f32[4096]{0:T(1024)S(1)} %convert_element_type.57, f32[8]{0:T(128)S(1)} %add_rsqrt_fusion.1), kind=kOutput, calls=%fused_computation.6 | convolution fusion | flops 134373376 | bytes 16990240 | tf_op jit(solution)/shard_map/dot_general | solution.py:74
  128.6 0.0 reduce-scatter.5.cloned.1.call-update
  128.6 53.0 %reduce-scatter.5.cloned.1.call-done = f32[8,256]{1,0:T(8,128)} async-done(((f32[8,4096]{1,0:T(8,128)}), f32[8,256]{1,0:T(8,128)}) %reduce-scatter.5.cloned.1.call-update) | async-done | bytes 8208 | tf_op jit(solution)/shard_map/reduce_scatter | solution.py:75
  181.6 1.3 add_convert_fusion
  (10 shorter events, 0.0 us)
Async XLA Ops:
  6.5 1.6 copy-start
  6.5 90.9 %reduce-scatter.3.cloned.1.call-start = ((), (), s32[]{:S(2)}) async-start(), calls=%async_computation.2 | async-start | bytes 40960 | tf_op jit(solution)/shard_map/reduce_scatter | solution.py:62
  30.5 4.0 %copy-start.1 = (f32[8,4,512]{2,1,0:T(4,128)S(1)}, f32[8,4,512]{2,1,0:T(4,128)}, u32[]{:S(2)}) copy-start(f32[8,4,512]{2,1,0:T(4,128)} %param.17) | copy-start | bytes 196612
  30.5 4.0 %copy-start.3 = (f32[64]{0:T(128)S(1)}, f32[64]{0:T(128)}, u32[]{:S(2)}) copy-start(f32[64]{0:T(128)} %param.14) | copy-start | bytes 772
  56.4 22.8 %copy-start.2 = (bf16[4096]{0:T(1024)(128)(2,1)S(1)}, bf16[4096]{0:T(1024)(128)(2,1)}, u32[]{:S(2)}) copy-start(bf16[4096]{0:T(1024)(128)(2,1)} %param.19) | copy-start | bytes 24580
  79.1 102.5 %reduce-scatter.5.cloned.1.call-start = ((), (), s32[]{:S(2)}) async-start(), calls=%async_computation.3 | async-start | bytes 139264 | tf_op jit(solution)/shard_map/reduce_scatter | solution.py:75
Sparse Core Ops, SparseCore 0:
  79.2 18.1 reduce-scatter.2
  128.8 52.8 reduce-scatter.4
where the time goes:
time: 190 us
  blocking collectives  74.5 us (39%)
  waiting for transfers between devices  71.2 us (37%)
  matrix products  17.9 us (9%)
  between operations  13.5 us (7%)
  local copies, waits for them, and re-layouts  9.15 us (5%)
  other arithmetic  3.46 us (2%)
    reduce_scatter x1, waiting for transfers between devices, per_device(): lax.psum_scatter(partials, ('kv', 'tp'), scatter_dimension=1, tiled=True)  53 us
    psum x1, blocking collectives, per_device(): query_raw = lax.psum(partial_value, 'kv')  20.8 us
    all_gather x1, blocking collectives, per_device(): lax.all_gather(residual, ('kv', 'tp'), axis=1, tiled=True)  20.6 us
    reduce_scatter x1, waiting for transfers between devices, per_device(): lax.psum_scatter(projected, 'tp', scatter_dimension=1, tiled=True)  18.2 us
    psum x1, blocking collectives, per_device(): lax.psum((factor * totals, factor[..., None] * weighted), 'kv')  17.6 us
    pmax x1, blocking collectives, per_device(): best = lax.pmax(score_top, 'kv')  15.5 us
    dot_general x1, matrix products, per_device(): partials = jnp.dot(squared, down_weight, preferred_element_type=jnp.float32)  9.78 us
    unnamed x10, local copies, waits for them, and re-layouts  8.7 us
  transfers between devices with their start and end apart: 2, of which 2 were waited for; matrix products, arithmetic and copies ran while one was open for 0% of the time, Pallas kernels for 0%

commit v1 on v0

--- a/solution.py
+++ b/solution.py
@@ -46,7 +46,11 @@
     batch_rows = stream.shape[0]
     scaled = (stream.astype(jnp.float32) * attn_gain.astype(jnp.float32)).astype(jnp.bfloat16)
     partial_value = jnp.dot(scaled, query_weight, preferred_element_type=jnp.float32)
-    query_raw = lax.psum(partial_value, "kv")
+    query_raw = partial_value
+    for hop in (1, 2):
+        query_raw = query_raw + lax.ppermute(
+            query_raw, "kv", [(dev, dev ^ hop) for dev in range(4)]
+        )
     kv_local = key_cache.shape[2] // HEAD_DIM
     heads_local = query_raw.shape[1] // HEAD_DIM
     query_heads = query_raw.reshape(batch_rows, heads_local, HEAD_DIM)

time: 190 us -> 179 us (0.942)
  blocking collectives: 74.5 us -> 54.6 us
  starting transfers between devices: 0.04 us -> 6.13 us
  waiting for transfers between devices: 71.2 us -> 73.7 us
    psum x1 -> x0, blocking collectives: 20.8 us -> none  [per_device(): query_raw = lax.psum(partial_value, 'kv')]
    ppermute x0 -> x2, starting transfers between devices: none -> 6.09 us  [per_device(): lax.ppermute(query_raw, 'kv', [(dev, dev ^ hop) for dev in range(4)])]
  transfers between devices with their start and end apart: 2 -> 4, of which waited for: 2 -> 3; matrix products, arithmetic and copies ran while one was open for 0% -> 4% of each run, Pallas kernels for 0% -> 0%
where the time goes in v1:
time: 179 us; the launch traced here: 178 us
  waiting for transfers between devices  73.7 us (41%)
  blocking collectives  54.6 us (31%)
  matrix products  17.9 us (10%)
  between operations  13.5 us (8%)
  local copies, waits for them, and re-layouts  9.14 us (5%)
  starting transfers between devices  6.13 us (3%)
  other arithmetic  3.47 us (2%)
    reduce_scatter x1, waiting for transfers between devices, per_device(): lax.psum_scatter(partials, ('kv', 'tp'), scatter_dimension=1, tiled=True)  53 us
    all_gather x1, blocking collectives, per_device(): lax.all_gather(residual, ('kv', 'tp'), axis=1, tiled=True)  20.6 us
    reduce_scatter x1, waiting for transfers between devices, per_device(): lax.psum_scatter(projected, 'tp', scatter_dimension=1, tiled=True)  18.8 us
    psum x1, blocking collectives, per_device(): lax.psum((factor * totals, factor[..., None] * weighted), 'kv')  17 us
    pmax x1, blocking collectives, per_device(): best = lax.pmax(score_top, 'kv')  17 us
    dot_general x1, matrix products, per_device(): partials = jnp.dot(squared, down_weight, preferred_element_type=jnp.float32)  9.78 us
    unnamed x10, local copies, waits for them, and re-layouts  8.7 us
    ppermute x2, starting transfers between devices, per_device(): lax.ppermute(query_raw, 'kv', [(dev, dev ^ hop) for dev in range(4)])  6.09 us
  transfers between devices with their start and end apart: 4, of which 3 were waited for; matrix products, arithmetic and copies ran while one was open for 4% of the time, Pallas kernels for 0%

profile of v1, /device:TPU:0, one launch (start us, length us, event | category | flops | bytes accessed | tf_op | source)
XLA Modules:
  0.0 178.4 jit_solution(12828232073183710899)
XLA Ops:
  6.5 0.8 convert_element_type.48
  7.4 0.8 copy-done
  8.1 1.1 fusion.19
  9.2 3.1 %collective-permute-start = (f32[8,1024]{1,0:T(8,128)S(1)}, f32[8,1024]{1,0:T(8,128)S(1)}, u32[]{:S(2)}, u32[]{:S(2)}) collective-permute-start(f32[8,1024]{1,0:T(8,128)S(1)} %fusion.19), channel_id=1, source_target_pairs={{0,4},{4,0},{8,12},{12,8},{1,5},{5,1},{9,13},{13,9},{2,6},{6,2},{1... | collective-permute-start | bytes 98312 | tf_op jit(solution)/shard_map/ppermute | solution.py:51
  12.3 1.9 %collective-permute-done = f32[8,1024]{1,0:T(8,128)S(1)} collective-permute-done((f32[8,1024]{1,0:T(8,128)S(1)}, f32[8,1024]{1,0:T(8,128)S(1)}, u32[]{:S(2)}, u32[]{:S(2)}) %collective-permute-start) | collective-permute-done | bytes 32800 | tf_op jit(solution)/shard_map/ppermute | solution.py:51
  14.2 3.0 %collective-permute-start.1 = (f32[8,1024]{1,0:T(8,128)S(1)}, f32[8,1024]{1,0:T(8,128)S(1)}, u32[]{:S(2)}, u32[]{:S(2)}) collective-permute-start(f32[8,1024]{1,0:T(8,128)S(1)} %add.44), channel_id=1, source_target_pairs={{0,8},{4,12},{8,0},{12,4},{1,9},{5,13},{9,1},{13,5},{2,10},{6,14},... | collective-permute-start | bytes 98312 | tf_op jit(solution)/shard_map/ppermute | solution.py:51
  17.2 3.9 %copy.20 = bf16[8,512,256]{1,2,0:T(8,128)(2,1)} copy(bf16[8,512,256]{2,1,0:T(8,128)(2,1)} %param.15) | data formatting | bytes 4194304 | tf_op args[4]
  21.2 4.0 %copy.21 = bf16[8,512,256]{1,2,0:T(8,128)(2,1)} copy(bf16[8,512,256]{2,1,0:T(8,128)(2,1)} %param.16) | data formatting | bytes 4194304 | tf_op args[5]
  25.2 0.1 mul.75
  25.2 0.1 reduce_sum.27
  25.3 0.1 copy.18
  25.4 0.1 copy.19
  25.5 0.1 reshape.45
  25.6 2.1 %fusion.25 = (f32[8,4,4]{2,1,0:T(4,128)S(1)}, f32[8,4,4,512]{3,2,1,0:T(4,128)S(1)}) fusion(f32[8,4,512]{2,1,0:T(4,128)S(1)} %copy-done.1, bf16[8,512,4,64]{1,3,2,0:T(8,128)(2,1)} %bitcast.15, f32[8,4,4,64]{3,2,1,0:T(4,128)S(1)} %reshape.45, f32[64]{0:T(128)S(1)} %copy-done.3, f32[8,4,4]{2,1,0:T(4,128)S(1)} %copy.19), kind=kOutput, calls=%fused_computation.34 | convolution fusion | flops 8609664 | bytes 2458880 | tf_op jit(solution)/shard_map/skgd,spkd->skgp/dot_general | solution.py:19
  27.8 17.0 %pmax.7 = f32[8,4,4]{2,1,0:T(4,128)S(1)} all-reduce(f32[8,4,4]{2,1,0:T(4,128)S(1)} %get-tuple-element.11), channel_id=1, replica_groups=mesh['grp'=2,'kv'=4,'tp'=4] {'kv'}, use_global_device_ids=true, to_apply=%region_2.0 | all-reduce | flops 128 | bytes 1024 | tf_op jit(solution)/shard_map/pmax | solution.py:60
  44.7 0.2 fusion.4
  45.0 0.0 copy-start.2
  45.0 2.3 %convolution_multiply_fusion.1 = f32[8,4,4,64]{3,2,1,0:T(4,128)S(1)} fusion(bf16[8,512,4,64]{1,3,2,0:T(8,128)(2,1)} %bitcast.16, f32[8,4,4,512]{3,2,1,0:T(4,128)S(1)} %get-tuple-element.12, f32[8,4,4]{2,1,0:T(4,128)S(1)} %get-tuple-element.11, f32[8,4,4]{2,1,0:T(4,128)S(1)} %bitcast.22), kind=kOutput, calls=%fused_computation.2 | convolution fusion | flops 8527872 | bytes 2393088 | tf_op jit(solution)/shard_map/skgp,spkd->skgd/dot_general | solution.py:24
  47.3 17.0 %all-reduce = (f32[8,4,4,64]{3,2,1,0:T(4,128)S(1)}, f32[8,4,4]{2,1,0:T(4,128)S(1)}) all-reduce(f32[8,4,4,64]{3,2,1,0:T(4,128)S(1)} %convolution_multiply_fusion.1, f32[8,4,4]{2,1,0:T(4,128)S(1)} %bitcast.18), channel_id=1, replica_groups=mesh['grp'=2,'kv'=4,'tp'=4] {'kv'}, use_global_device_ids=true, to_apply=%region_3.0 | all-reduce | flops 8320 | bytes 66560 | tf_op jit(solution)/shard_map/psum | solution.py:62
  64.4 0.1 divide_convert_fusion
  64.5 0.1 convert_element_type.53
  64.6 2.6 %fusion.26 = f32[8,1024]{1,0:T(8,128)} fusion(bf16[8,1024]{1,0:T(8,128)(2,1)S(1)} %convert_element_type.53, bf16[1024,1024]{1,0:T(8,128)(2,1)} %param.18), kind=kOutput, calls=%fused_computation.35 | convolution fusion | flops 16777216 | bytes 2146304 | tf_op jit(solution)/shard_map/dot_general | solution.py:65
  67.1 0.0 reduce-scatter.3.cloned.1.call-update
  67.2 0.0 reduce-scatter.5.cloned.1.call-start
  67.2 18.8 %reduce-scatter.3.cloned.1.call-done = f32[8,256]{1,0:T(8,128)} async-done(((f32[8,1024]{1,0:T(8,128)}), f32[8,256]{1,0:T(8,128)}) %reduce-scatter.3.cloned.1.call-update) | async-done | bytes 8208 | tf_op jit(solution)/shard_map/reduce_scatter | solution.py:66
  86.0 0.7 add_convert_fusion.1
  86.7 20.6 %all_gather.3 = bf16[8,4096]{1,0:T(8,128)(2,1)S(1)} all-gather(bf16[8,256]{1,0:T(8,128)(2,1)S(1)} %add_convert_fusion.1), channel_id=1, replica_groups=mesh['grp'=2,'kv'=4,'tp'=4] {'kv','tp'}, dimensions={1}, use_global_device_ids=true | all-gather | bytes 69632 | tf_op jit(solution)/shard_map/all_gather | solution.py:70
  107.3 0.1 fusion.6
  107.5 9.8 %fusion.3 = f32[8,4096]{1,0:T(8,128)} fusion(bf16[1024,4096]{1,0:T(8,128)(2,1)} %param.21, bf16[1024,4096]{1,0:T(8,128)(2,1)} %param.20, bf16[8,4096]{1,0:T(8,128)(2,1)S(1)} %all_gather.3, f32[4096]{0:T(1024)S(1)} %convert_element_type.57, f32[8]{0:T(128)S(1)} %add_rsqrt_fusion.1), kind=kOutput, calls=%fused_computation.6 | convolution fusion | flops 134373376 | bytes 16990240 | tf_op jit(solution)/shard_map/dot_general | solution.py:78
  117.2 0.0 reduce-scatter.5.cloned.1.call-update
  117.3 53.0 %reduce-scatter.5.cloned.1.call-done = f32[8,256]{1,0:T(8,128)} async-done(((f32[8,4096]{1,0:T(8,128)}), f32[8,256]{1,0:T(8,128)}) %reduce-scatter.5.cloned.1.call-update) | async-done | bytes 8208 | tf_op jit(solution)/shard_map/reduce_scatter | solution.py:79
  170.2 1.3 add_convert_fusion
  (14 shorter events, 0.1 us)
Async XLA Ops:
  6.5 1.6 copy-start
  6.5 79.5 %reduce-scatter.3.cloned.1.call-start = ((), (), s32[]{:S(2)}) async-start(), calls=%async_computation.2 | async-start | bytes 40960 | tf_op jit(solution)/shard_map/reduce_scatter | solution.py:66
  9.2 4.9 %collective-permute-start = (f32[8,1024]{1,0:T(8,128)S(1)}, f32[8,1024]{1,0:T(8,128)S(1)}, u32[]{:S(2)}, u32[]{:S(2)}) collective-permute-start(f32[8,1024]{1,0:T(8,128)S(1)} %fusion.19), channel_id=1, source_target_pairs={{0,4},{4,0},{8,12},{12,8},{1,5},{5,1},{9,13},{13,9},{2,6},{6,2},{1... | collective-permute-start | bytes 98312 | tf_op jit(solution)/shard_map/ppermute | solution.py:51
  14.2 11.0 %collective-permute-start.1 = (f32[8,1024]{1,0:T(8,128)S(1)}, f32[8,1024]{1,0:T(8,128)S(1)}, u32[]{:S(2)}, u32[]{:S(2)}) collective-permute-start(f32[8,1024]{1,0:T(8,128)S(1)} %add.44), channel_id=1, source_target_pairs={{0,8},{4,12},{8,0},{12,4},{1,9},{5,13},{9,1},{13,5},{2,10},{6,14},... | collective-permute-start | bytes 98312 | tf_op jit(solution)/shard_map/ppermute | solution.py:51
  21.2 4.5 %copy-start.1 = (f32[8,4,512]{2,1,0:T(4,128)S(1)}, f32[8,4,512]{2,1,0:T(4,128)}, u32[]{:S(2)}) copy-start(f32[8,4,512]{2,1,0:T(4,128)} %param.17) | copy-start | bytes 196612
  21.2 4.5 %copy-start.3 = (f32[64]{0:T(128)S(1)}, f32[64]{0:T(128)}, u32[]{:S(2)}) copy-start(f32[64]{0:T(128)} %param.14) | copy-start | bytes 772
  45.0 22.2 %copy-start.2 = (bf16[4096]{0:T(1024)(128)(2,1)S(1)}, bf16[4096]{0:T(1024)(128)(2,1)}, u32[]{:S(2)}) copy-start(bf16[4096]{0:T(1024)(128)(2,1)} %param.19) | copy-start | bytes 24580
  67.2 103.1 %reduce-scatter.5.cloned.1.call-start = ((), (), s32[]{:S(2)}) async-start(), calls=%async_computation.3 | async-start | bytes 139264 | tf_op jit(solution)/shard_map/reduce_scatter | solution.py:79
Sparse Core Ops, SparseCore 0:
  67.3 18.6 reduce-scatter.2
  117.4 52.8 reduce-scatter.4
